TPU v7x, 32 devices: a whole 2x2x4 slice. The times are simulated.
32 devices in a mesh: fs: 16 (over z, y, x), tp: 2 (over core).
Axes of the slice: x: 2, y: 2, z: 4, core: 2. Of those that a mesh axis runs over, the one named last changes fastest.
Arguments:
- tokens: bfloat16 [4096, 2048], P('fs'), may hold values from -6 to 6
- routes: int32 [4096, 6], P('fs'), may hold values from 0 to 15, all different within a row; in each aligned block of 256 rows (0 to 255, 256 to 511, ...) at most 160 rows name the same one
- route_weights: float32 [4096, 6], P('fs'), may hold values from 0.1 to 1
- norm_gain: float32 [2048], P('fs'), may hold values from 0.1 to 1.9
- expert_gate: float32 [16, 2048, 1024], P(None, 'fs', 'tp'), may hold values from -0.125 to 0.125
- expert_up: float32 [16, 2048, 1024], P(None, 'fs', 'tp'), may hold values from -0.125 to 0.125
- expert_down: float32 [16, 2048, 1024], P(None, 'fs', 'tp'), may hold values from -0.1875 to 0.1875
- shared_gate: float32 [2048, 1024], P('fs', 'tp'), may hold values from -0.125 to 0.125
- shared_up: float32 [2048, 1024], P('fs', 'tp'), may hold values from -0.125 to 0.125
- shared_down: float32 [2048, 1024], P('fs', 'tp'), may hold values from -0.1875 to 0.1875
Outputs:
- layer_output: bfloat16 [4096, 2048], P('fs', 'tp')
- sample_gate: bfloat16 [16, 2048, 1024], P('fs', None, 'tp')
- sample_up: bfloat16 [16, 2048, 1024], P('fs', None, 'tp')
- sample_down: bfloat16 [16, 2048, 1024], P('fs', None, 'tp')
- common_gate: bfloat16 [2048, 1024], P(None, 'tp')
- common_up: bfloat16 [2048, 1024], P(None, 'tp')
- common_down: bfloat16 [2048, 1024], P(None, 'tp')
Inputs may be any that keep to these rules, and one draw needn't show every extreme that they name: `routes`: each row names 6 different experts. In each aligned block of 256 rows (the rows of one index of fs) no expert is named by more than 160 rows, a bound that some expert reaches in some blocks.
All inputs are finite; a program needn't handle non-finite values.
Results may differ from a plain program's by a relative error of at most 0.015.
Values may be sent and summed in bfloat16 or wider, within the bound.
A program may use at most 128 MiB of HBM per device.

v0:
```python
import jax
import jax.numpy as jnp
from jax import lax
from jax.sharding import PartitionSpec as P

EPSILON = 1e-06


def normalize(tokens):
    values = tokens.astype(jnp.float32)
    scale = lax.rsqrt(jnp.mean(values * values, axis=-1, keepdims=True) + EPSILON)
    return (values * scale).astype(jnp.bfloat16)


def ring_of(fs_count):
    if fs_count != 16:
        return list(range(fs_count))
    order = []
    for place, column in enumerate((0, 1, 3, 2)):
        heights = range(4) if place % 2 == 0 else range(3, -1, -1)
        order.extend((height * 4 + column for height in heights))
    return order


def reorder(blocks, order):
    if list(order) == list(range(len(order))):
        return blocks
    return jnp.concatenate([blocks[i : i + 1] for i in order], axis=0)


def body(
    tokens,
    routes,
    route_weights,
    norm_gain,
    expert_gate,
    expert_up,
    expert_down,
    shared_gate,
    shared_up,
    shared_down,
):
    tp_count = lax.axis_size("tp")
    tp_index = lax.axis_index("tp")
    fs_count = lax.axis_size("fs")
    tok_rows, width = tokens.shape
    experts = expert_gate.shape[0]
    share = tok_rows // tp_count
    own_experts = experts // fs_count
    ring = ring_of(fs_count)
    place_of = [ring.index(i) for i in range(fs_count)]
    groups = None if ring == list(range(fs_count)) else [ring]
    normed = normalize(tokens)
    own_normed = lax.dynamic_slice_in_dim(normed, tp_index * share, share, 0)
    own_routes = lax.dynamic_slice_in_dim(routes, tp_index * share, share, 0)
    own_weights = lax.dynamic_slice_in_dim(route_weights, tp_index * share, share, 0)
    member = own_routes[None, :, :] == jnp.arange(experts, dtype=jnp.int32)[:, None, None]
    dense = jnp.sum(jnp.where(member, own_weights[None, :, :], 0.0), axis=2)
    dense_all = lax.all_gather(dense, "fs", axis=0, tiled=False)
    own_normed, dense_all = lax.optimization_barrier((own_normed, dense_all))
    gathered = lax.all_gather(own_normed, "fs", axis=0, tiled=False)
    gathered = reorder(gathered, ring).reshape(fs_count * share, width)
    gain_rows = norm_gain[None, :, None]
    rounded = (
        (expert_gate * gain_rows).astype(jnp.bfloat16),
        (expert_up * gain_rows).astype(jnp.bfloat16),
        expert_down.astype(jnp.bfloat16),
    )
    sample_gate, sample_up, sample_down = (
        lax.all_to_all(rounded[0], "fs", split_axis=0, concat_axis=1, tiled=True),
        lax.all_to_all(rounded[1], "fs", split_axis=0, concat_axis=1, tiled=True),
        lax.all_to_all(rounded[2], "fs", split_axis=0, concat_axis=1, tiled=True),
    )
    half = shared_gate.shape[1]
    shared_rows = jnp.concatenate(
        [
            (shared_gate * norm_gain[:, None]).astype(jnp.bfloat16),
            (shared_up * norm_gain[:, None]).astype(jnp.bfloat16),
            shared_down.astype(jnp.bfloat16),
        ],
        axis=1,
    )
    common = lax.all_gather(shared_rows, "fs", axis=0, tiled=False, axis_index_groups=groups)
    common_gate, common_up, common_down = (
        reorder(common[:, :, i * half : (i + 1) * half], place_of).reshape(width, half)
        for i in range(3)
    )
    shared_gate_act = jnp.dot(normed, common_gate, preferred_element_type=jnp.float32)
    shared_up_act = jnp.dot(normed, common_up, preferred_element_type=jnp.float32)
    shared_hidden = (jax.nn.silu(shared_gate_act) * shared_up_act).astype(jnp.bfloat16)
    shared_part = jnp.einsum(
        "th,dh->td", shared_hidden, common_down, preferred_element_type=jnp.float32
    ).astype(jnp.bfloat16)
    shared_parts = lax.all_to_all(
        shared_part.reshape(tok_rows, tp_count, width // tp_count).transpose(1, 0, 2),
        "tp",
        split_axis=0,
        concat_axis=0,
        tiled=True,
    )
    shared_sum = jnp.sum(shared_parts.astype(jnp.float32), axis=0)
    scale_all = reorder(
        lax.dynamic_slice_in_dim(dense_all, lax.axis_index("fs") * own_experts, own_experts, 1),
        ring,
    )
    total = None
    for expert in range(own_experts):
        scale = scale_all[:, expert, :].reshape(-1)[:, None]
        for shift in range(tp_count):
            gate_w, up_w, down_w = (sample_gate[expert], sample_up[expert], sample_down[expert])
            if shift:
                pairs = [(i, (i + shift) % tp_count) for i in range(tp_count)]
                gate_w, up_w, down_w = (
                    lax.ppermute(gate_w, "tp", pairs),
                    lax.ppermute(up_w, "tp", pairs),
                    lax.ppermute(down_w, "tp", pairs),
                )
            gate = jnp.dot(gathered, gate_w, preferred_element_type=jnp.float32)
            upward = jnp.dot(gathered, up_w, preferred_element_type=jnp.float32)
            hidden = (jax.nn.silu(gate) * upward * scale).astype(jnp.bfloat16)
            part = jnp.einsum("rf,df->rd", hidden, down_w, preferred_element_type=jnp.float32)
            total = part if total is None else total + part
    routed = lax.psum_scatter(
        total.astype(jnp.bfloat16), "fs", scatter_dimension=0, tiled=True, axis_index_groups=groups
    )
    routed = lax.all_to_all(routed, "tp", split_axis=1, concat_axis=0, tiled=True)
    layer_output = (routed.astype(jnp.float32) + shared_sum).astype(jnp.bfloat16)
    return (layer_output, sample_gate, sample_up, sample_down, common_gate, common_up, common_down)


def solution(mesh):
    return jax.shard_map(
        body,
        mesh=mesh,
        in_specs=(
            P("fs", None),
            P("fs", None),
            P("fs", None),
            P("fs"),
            P(None, "fs", "tp"),
            P(None, "fs", "tp"),
            P(None, "fs", "tp"),
            P("fs", "tp"),
            P("fs", "tp"),
            P("fs", "tp"),
        ),
        out_specs=(
            P("fs", "tp"),
            P("fs", None, "tp"),
            P("fs", None, "tp"),
            P("fs", None, "tp"),
            P(None, "tp"),
            P(None, "tp"),
            P(None, "tp"),
        ),
        check_vma=False,
    )
```

profile of v0, /device:TPU:0, one launch (start us, length us, event | category | flops | bytes accessed | tf_op | source)
XLA Modules:
  0.0 481.2 jit_solution(11208492477389067535)
XLA Ops:
  8.6 43.1 %all-gather = f32[256,128]{1,0:T(8,128)S(1)} all-gather(f32[16,128]{1,0:T(8,128)S(1)} %select_reduce_fusion), channel_id=2, replica_groups=mesh['fs'=16,'tp'=2] {'fs'}, dimensions={0}, use_global_device_ids=true | all-gather | bytes 139264 | tf_op jit(solution)/shard_map/all_gather | solution.py:59
  51.7 1.5 fusion
  53.2 1.5 fusion.1
  55.5 6.1 %multiply_convert_fusion.2 = (bf16[16,128,512]{2,1,0:T(8,128)(2,1)}, bf16[16,128,512]{2,1,0:T(8,128)(2,1)S(1)}) fusion(f32[16,128,512]{2,1,0:T(8,128)} %param.15, f32[128]{0:T(128)S(1)} %copy-done.8, f32[16,128,512]{2,1,0:T(8,128)} %param.14), kind=kLoop, calls=%fused_computation.3 | loop fusion | flops 4194304 | bytes 12583424 | tf_op jit(solution)/shard_map/convert_element_type | solution.py:66
  61.7 78.2 %all_to_all.54 = bf16[16,128,512]{2,1,0:T(8,128)(2,1)S(1)} all-to-all(bf16[16,128,512]{2,1,0:T(8,128)(2,1)S(1)} %get-tuple-element.57), channel_id=1, replica_groups=mesh['fs'=16,'tp'=2] {'fs'}, dimensions={0} | all-to-all | bytes 4194304 | tf_op jit(solution)/shard_map/all_to_all | solution.py:70
  139.9 4.5 all-to-all-start.1
  144.4 3.8 convert_element_type.59
  148.2 68.6 %all-to-all-done.1 = bf16[16,128,512]{2,1,0:T(8,128)(2,1)} async-done(((bf16[16,128,512]{2,1,0:T(8,128)(2,1)}), bf16[16,128,512]{2,1,0:T(8,128)(2,1)}, u32[]{:S(2)}, u32[]{:S(2)}) %all-to-all-start.1) | async-done | bytes 2097184 | tf_op jit(solution)/shard_map/all_to_all | solution.py:71
  216.8 22.6 %all-to-all-start.2 = ((bf16[16,128,512]{2,1,0:T(8,128)(2,1)}), bf16[16,128,512]{2,1,0:T(8,128)(2,1)}, u32[]{:S(2)}, u32[]{:S(2)}) async-start(bf16[16,128,512]{2,1,0:T(8,128)(2,1)} %convert_element_type.59), calls=%async_computation.2 | async-start | bytes 4194304 | tf_op jit(solution)/shard_map/all_to_all | solution.py:72
  239.4 1.1 multiply_convert_fusion.6
  242.5 57.3 %all-to-all-done.2 = bf16[16,128,512]{2,1,0:T(8,128)(2,1)} async-done(((bf16[16,128,512]{2,1,0:T(8,128)(2,1)}), bf16[16,128,512]{2,1,0:T(8,128)(2,1)}, u32[]{:S(2)}, u32[]{:S(2)}) %all-to-all-start.2) | async-done | bytes 2097184 | tf_op jit(solution)/shard_map/all_to_all | solution.py:72
  300.9 1.2 fusion.19
  302.1 1.8 fusion.18
  304.0 1.1 fusion.17
  305.1 1.1 fusion.16
  307.7 6.0 %fusion.30 = f32[2048,512]{1,0:T(8,128)} fusion(bf16[2048,2048]{1,0:T(8,128)(2,1)S(1)} %bitcast.140, bf16[2048,512]{1,0:T(8,128)(2,1)S(1)} %bitcast.104), kind=kOutput, calls=%fused_computation.142 | convolution fusion | flops 4294967296 | bytes 14680064 | tf_op jit(solution)/shard_map/dot_general | solution.py:118
  313.7 7.6 %fusion.31 = f32[2048,512]{1,0:T(8,128)} fusion(bf16[2048,2048]{1,0:T(8,128)(2,1)S(1)} %bitcast.141, bf16[2048,512]{1,0:T(8,128)(2,1)} %collective-permute-done), kind=kOutput, calls=%fused_computation.143 | convolution fusion | flops 4294967296 | bytes 14680064 | tf_op jit(solution)/shard_map/dot_general | solution.py:118
  321.3 7.6 %fusion.32 = f32[2048,512]{1,0:T(8,128)} fusion(bf16[2048,2048]{1,0:T(8,128)(2,1)S(1)} %bitcast.142, bf16[2048,512]{1,0:T(8,128)(2,1)} %collective-permute-done.1), kind=kOutput, calls=%fused_computation.144 | convolution fusion | flops 4294967296 | bytes 14680064 | tf_op jit(solution)/shard_map/dot_general | solution.py:119
  328.9 16.7 %fusion.6 = f32[2048,2048]{1,0:T(8,128)} fusion(bf16[2048,512]{1,0:T(8,128)(2,1)} %bitcast.20, f32[2048,512]{1,0:T(8,128)} %fusion.30, bf16[2048,2048]{1,0:T(8,128)(2,1)} %bitcast.143, bf16[2048,512]{1,0:T(8,128)(2,1)} %bitcast.18, f32[2048]{0:T(1024)S(1)} %bitcast.150), kind=kOutput, calls=%fused_computation.18 | convolution fusion | flops 8597274624 | bytes 33562624 | tf_op jit(solution)/shard_map/rf,df->rd/dot_general | solution.py:121
  345.6 13.5 %add_convert_fusion = bf16[2048,2048]{1,0:T(8,128)(2,1)} fusion(f32[2048,2048]{1,0:T(8,128)} %fusion.6, bf16[2048,512]{1,0:T(8,128)(2,1)} %collective-permute-done.2, f32[2048,512]{1,0:T(8,128)} %fusion.32, f32[2048,512]{1,0:T(8,128)} %fusion.31, f32[2048]{0:T(1024)S(1)} %bitcast.151), kind=kOutput, calls=%fused_computation | convolution fusion | flops 4310695936 | bytes 35659776 | tf_op jit(solution)/shard_map/rf,df->rd/dot_general | solution.py:121
  371.9 1.2 slice_dynamic-update-slice_fusion.2
  373.1 1.2 constant_dynamic-update-slice_fusion.17
  375.4 1.3 copy-done.5
  376.7 1.5 fusion.33
  378.2 4.8 convolution_convert_fusion
  383.0 1.3 copy.30
  384.3 4.6 all_to_all.55
  389.1 71.9 %reduce-scatter.2.cloned.1.call-done = bf16[128,2048]{1,0:T(8,128)(2,1)} async-done(((bf16[2048,2048]{1,0:T(8,128)(2,1)}), bf16[128,2048]{1,0:T(8,128)(2,1)}) %reduce-scatter.2.cloned.1.call-update) | async-done | bytes 524304 | tf_op jit(solution)/shard_map/reduce_scatter | solution.py:123
  462.1 4.2 all_to_all.56
  467.2 1.3 copy.105
  468.5 3.1 copy.106
  471.6 3.0 copy.107
  (82 shorter events, 22.9 us)
Async XLA Ops:
  7.2 0.7 copy-start
  7.2 292.6 %all-gather.6.cloned.1.call-start = ((), (), s32[]{:S(2)}) async-start(), calls=%async_computation.7 | async-start | bytes 8912896 | tf_op jit(solution)/shard_map/all_gather | solution.py:61
  53.2 2.4 copy-start.8
  139.9 76.9 %all-to-all-start.1 = ((bf16[16,128,512]{2,1,0:T(8,128)(2,1)}), bf16[16,128,512]{2,1,0:T(8,128)(2,1)}, u32[]{:S(2)}, u32[]{:S(2)}) async-start(bf16[16,128,512]{2,1,0:T(8,128)(2,1)} %get-tuple-element.56), calls=%async_computation.1 | async-start | bytes 4194304 | tf_op jit(solution)/shard_map/all_to_all | solution.py:71
  148.2 91.2 %copy-start.3 = (f32[128,512]{1,0:T(8,128)S(1)}, f32[128,512]{1,0:T(8,128)}, u32[]{:S(2)}) copy-start(f32[128,512]{1,0:T(8,128)} %param.19) | copy-start | bytes 786436
  216.8 83.0 %all-to-all-start.2 = ((bf16[16,128,512]{2,1,0:T(8,128)(2,1)}), bf16[16,128,512]{2,1,0:T(8,128)(2,1)}, u32[]{:S(2)}, u32[]{:S(2)}) async-start(bf16[16,128,512]{2,1,0:T(8,128)(2,1)} %convert_element_type.59), calls=%async_computation.2 | async-start | bytes 4194304 | tf_op jit(solution)/shard_map/all_to_all | solution.py:72
  239.4 119.8 %all-gather.8.cloned.1.call-start = ((), (), s32[]{:S(2)}) async-start(), calls=%async_computation.8 | async-start | bytes 6684672 | tf_op jit(solution)/shard_map/all_gather | solution.py:83
  241.4 219.7 %reduce-scatter.2.cloned.1.call-start = ((), (), s32[]{:S(2)}) async-start(), calls=%async_computation.6 | async-start | bytes 8912896 | tf_op jit(solution)/shard_map/reduce_scatter | solution.py:123
  241.9 71.8 %collective-permute-start = (bf16[2048,512]{1,0:T(8,128)(2,1)S(1)}, bf16[2048,512]{1,0:T(8,128)(2,1)}, u32[]{:S(2)}, u32[]{:S(2)}) collective-permute-start(bf16[2048,512]{1,0:T(8,128)(2,1)S(1)} %bitcast.103), channel_id=1, source_target_pairs={{0,1},{1,0},{2,3},{3,2},{4,5},{5,4},{6,7},{7,6},{8,9},{9,8},{10,11... | collective-permute-start | bytes 6291464 | tf_op jit(solution)/shard_map/ppermute | solution.py:114
  242.0 79.3 %collective-permute-start.1 = (bf16[2048,512]{1,0:T(8,128)(2,1)}, bf16[2048,512]{1,0:T(8,128)(2,1)}, u32[]{:S(2)}, u32[]{:S(2)}) collective-permute-start(bf16[2048,512]{1,0:T(8,128)(2,1)} %bitcast.18), channel_id=1, source_target_pairs={{0,1},{1,0},{2,3},{3,2},{4,5},{5,4},{6,7},{7,6},{8,9},{9,8},{10,11... | collective-permute-start | bytes 6291464 | tf_op jit(solution)/shard_map/ppermute | solution.py:115
  299.8 45.8 %collective-permute-start.2 = (bf16[2048,512]{1,0:T(8,128)(2,1)}, bf16[2048,512]{1,0:T(8,128)(2,1)}, u32[]{:S(2)}, u32[]{:S(2)}) collective-permute-start(bf16[2048,512]{1,0:T(8,128)(2,1)} %bitcast.20), channel_id=1, source_target_pairs={{0,1},{1,0},{2,3},{3,2},{4,5},{5,4},{6,7},{7,6},{8,9},{9,8},{10,11... | collective-permute-start | bytes 6291464 | tf_op jit(solution)/shard_map/ppermute | solution.py:116
  300.8 3.1 slice-start
  300.8 6.4 %copy-start.2 = (bf16[2048,2048]{1,0:T(8,128)(2,1)S(1)}, bf16[2048,2048]{1,0:T(8,128)(2,1)}, u32[]{:S(2)}) copy-start(bf16[2048,2048]{1,0:T(8,128)(2,1)} %all-gather.6.cloned.1.call-done) | copy-start | bytes 25165828
  307.7 13.6 %copy-start.4 = (bf16[16,128,2048]{2,1,0:T(8,128)(2,1)}, bf16[16,128,2048]{2,1,0:T(8,128)(2,1)S(1)}, u32[]{:S(2)}) copy-start(bf16[16,128,2048]{2,1,0:T(8,128)(2,1)S(1)} %fusion.7) | copy-start | bytes 25165828
  375.4 1.3 copy-start.5
  375.4 2.8 copy-start.6
  375.4 2.8 copy-start.7
  468.5 6.1 %copy-start.1 = (f32[256,6]{0,1:T(8,128)S(1)}, f32[256,6]{0,1:T(8,128)}, u32[]{:S(2)}) copy-start(f32[256,6]{0,1:T(8,128)} %param.12) | copy-start | bytes 18436
Sparse Core Ops, SparseCore 0:
  55.7 179.2 all-gather.5
  242.3 108.1 all-gather.7
  359.2 101.7 reduce-scatter.1
where the time goes:
time: 482 us; the launch traced here: 481 us
  waiting for transfers between devices  198 us (41%)
  blocking collectives  130 us (27%)
  matrix products  57.7 us (12%)
  local copies, waits for them, and re-layouts  37.5 us (8%)
  starting transfers between devices  27.9 us (6%)
  other arithmetic  16 us (3%)
  between operations  14.1 us (3%)
    all_to_all x1, blocking collectives, body(): lax.all_to_all(rounded[0], 'fs', split_axis=0, concat_axis=1, tiled=True)  78.2 us
    reduce_scatter x1, waiting for transfers between devices, body(): lax.psum_scatter(total.astype(jnp.bfloat16), 'fs', scatter_dimension=0, t...  71.9 us
    all_to_all x1, waiting for transfers between devices, body(): lax.all_to_all(rounded[1], 'fs', split_axis=0, concat_axis=1, tiled=True)  68.6 us
    all_to_all x1, waiting for transfers between devices, body(): lax.all_to_all(rounded[2], 'fs', split_axis=0, concat_axis=1, tiled=True)  57.3 us
    all_gather x1, blocking collectives, body(): dense_all = lax.all_gather(dense, 'fs', axis=0, tiled=False)  43.1 us
    unnamed x63, local copies, waits for them, and re-layouts  32.5 us
    dot_general x2, matrix products, body(): jnp.einsum('rf,df->rd', hidden, down_w, preferred_element_type=jnp.float32)  30.2 us
    all_to_all x1, starting transfers between devices, body(): lax.all_to_all(rounded[2], 'fs', split_axis=0, concat_axis=1, tiled=True)  22.6 us
  transfers between devices with their start and end apart: 8, of which 3 were waited for; matrix products, arithmetic and copies ran while one was open for 20% of the time, Pallas kernels for 0%

commit v1 on v0

--- a/solution.py
+++ b/solution.py
@@ -68,7 +68,12 @@
     )
     sample_gate, sample_up, sample_down = (
         lax.all_to_all(rounded[0], "fs", split_axis=0, concat_axis=1, tiled=True),
-        lax.all_to_all(rounded[1], "fs", split_axis=0, concat_axis=1, tiled=True),
+        jnp.concatenate(
+            lax.all_to_all(
+                jnp.stack(jnp.split(rounded[1], lax.axis_size("fs"), axis=0)), "fs", 0, 0
+            ),
+            axis=1,
+        ),
         lax.all_to_all(rounded[2], "fs", split_axis=0, concat_axis=1, tiled=True),
     )
     half = shared_gate.shape[1]

time: 482 us -> 487 us (1.010)
  blocking collectives: 130 us -> 51.9 us
  waiting for transfers between devices: 198 us -> 251 us
  starting transfers between devices: 27.9 us -> 44.2 us
  local copies, waits for them, and re-layouts: 37.5 us -> 48.1 us
    all_to_all x1 -> x0, blocking collectives: 78.2 us -> none  [body(): lax.all_to_all(rounded[0], 'fs', split_axis=0, concat_axis=1, tiled=True)]
    all_to_all x1 -> x2, waiting for transfers between devices: 68.6 us -> 123 us  [the longest x1 68.5 us: body(): lax.all_to_all(jnp.stack(jnp.split(rounded[1], lax.axis_size('fs'), axis=...]
    all_to_all x1 -> x2, starting transfers between devices: 4.49 us -> 19.3 us  [the longest x1 14.9 us: body(): lax.all_to_all(jnp.stack(jnp.split(rounded[1], lax.axis_size('fs'), axis=...]
    unnamed x63 -> x78, local copies, waits for them, and re-layouts: 32.5 us -> 42.4 us
  transfers between devices with their start and end apart: 8 -> 9, of which waited for: 3 -> 4; matrix products, arithmetic and copies ran while one was open for 20% -> 22% of each run, Pallas kernels for 0% -> 0%
where the time goes in v1:
time: 487 us; the launch traced here: 486 us
  waiting for transfers between devices  251 us (52%)
  matrix products  60.2 us (12%)
  blocking collectives  51.9 us (11%)
  local copies, waits for them, and re-layouts  48.1 us (10%)
  starting transfers between devices  44.2 us (9%)
  other arithmetic  16.3 us (3%)
  between operations  14.1 us (3%)
    reduce_scatter x1, waiting for transfers between devices, body(): lax.psum_scatter(total.astype(jnp.bfloat16), 'fs', scatter_dimension=0, t...  71.6 us
    all_to_all x1, waiting for transfers between devices, body(): lax.all_to_all(jnp.stack(jnp.split(rounded[1], lax.axis_size('fs'), axis=...  68.5 us
    all_to_all x1, waiting for transfers between devices, body(): lax.all_to_all(rounded[2], 'fs', split_axis=0, concat_axis=1, tiled=True)  56.9 us
    all_to_all x1, waiting for transfers between devices, body(): lax.all_to_all(rounded[0], 'fs', split_axis=0, concat_axis=1, tiled=True)  54.2 us
    all_gather x1, blocking collectives, body(): dense_all = lax.all_gather(dense, 'fs', axis=0, tiled=False)  43.1 us
    unnamed x78, local copies, waits for them, and re-layouts  42.4 us
    dot_general x2, matrix products, body(): jnp.einsum('rf,df->rd', hidden, down_w, preferred_element_type=jnp.float32)  29.6 us
    all_to_all x1, starting transfers between devices, body(): lax.all_to_all(rounded[2], 'fs', split_axis=0, concat_axis=1, tiled=True)  24 us
  transfers between devices with their start and end apart: 9, of which 4 were waited for; matrix products, arithmetic and copies ran while one was open for 22% of the time, Pallas kernels for 0%

profile of v1, /device:TPU:0, one launch (start us, length us, event | category | flops | bytes accessed | tf_op | source)
XLA Modules:
  0.0 486.1 jit_solution(1355189986930438486)
XLA Ops:
  8.6 43.1 %all-gather = f32[256,128]{1,0:T(8,128)S(1)} all-gather(f32[16,128]{1,0:T(8,128)S(1)} %select_reduce_fusion), channel_id=2, replica_groups=mesh['fs'=16,'tp'=2] {'fs'}, dimensions={0}, use_global_device_ids=true | all-gather | bytes 139264 | tf_op jit(solution)/shard_map/all_gather | solution.py:59
  51.7 1.5 fusion
  53.2 1.5 fusion.1
  55.5 6.1 %multiply_convert_fusion.2 = (bf16[16,128,512]{2,1,0:T(8,128)(2,1)S(1)}, bf16[16,128,512]{2,1,0:T(8,128)(2,1)}) fusion(f32[16,128,512]{2,1,0:T(8,128)} %param.15, f32[128]{0:T(128)S(1)} %copy-done.8, f32[16,128,512]{2,1,0:T(8,128)} %param.14), kind=kLoop, calls=%fused_computation.3 | loop fusion | flops 4194304 | bytes 12583424 | tf_op jit(solution)/shard_map/convert_element_type | solution.py:66
  61.7 4.4 all-to-all-start
  76.7 54.2 %all-to-all-done = bf16[16,128,512]{2,1,0:T(8,128)(2,1)} async-done(((bf16[16,128,512]{2,1,0:T(8,128)(2,1)}), bf16[16,128,512]{2,1,0:T(8,128)(2,1)}, u32[]{:S(2)}, u32[]{:S(2)}) %all-to-all-start) | async-done | bytes 2097184 | tf_op jit(solution)/shard_map/all_to_all | solution.py:70
  130.9 14.9 %all-to-all-start.1 = ((bf16[16,1,128,512]{3,2,1,0:T(8,128)(2,1)}), bf16[16,1,128,512]{3,2,1,0:T(8,128)(2,1)S(1)}, u32[]{:S(2)}, u32[]{:S(2)}) async-start(bf16[16,1,128,512]{3,2,1,0:T(8,128)(2,1)} %constant_dynamic-update-slice_fusion.1), calls=%async_computation.1 | async-start | bytes 4194304 | tf_op jit(solution)/shard_map/all_to_all | solution.py:72
  145.8 4.1 convert_element_type.59
  149.9 68.5 %all-to-all-done.1 = bf16[16,1,128,512]{3,2,1,0:T(8,128)(2,1)S(1)} async-done(((bf16[16,1,128,512]{3,2,1,0:T(8,128)(2,1)}), bf16[16,1,128,512]{3,2,1,0:T(8,128)(2,1)S(1)}, u32[]{:S(2)}, u32[]{:S(2)}) %all-to-all-start.1) | async-done | bytes 2097184 | tf_op jit(solution)/shard_map/all_to_all | solution.py:72
  218.4 24.0 %all-to-all-start.2 = ((bf16[16,128,512]{2,1,0:T(8,128)(2,1)}), bf16[16,128,512]{2,1,0:T(8,128)(2,1)}, u32[]{:S(2)}, u32[]{:S(2)}) async-start(bf16[16,128,512]{2,1,0:T(8,128)(2,1)} %convert_element_type.59), calls=%async_computation.2 | async-start | bytes 4194304 | tf_op jit(solution)/shard_map/all_to_all | solution.py:77
  242.5 1.1 multiply_convert_fusion.6
  245.6 56.9 %all-to-all-done.2 = bf16[16,128,512]{2,1,0:T(8,128)(2,1)} async-done(((bf16[16,128,512]{2,1,0:T(8,128)(2,1)}), bf16[16,128,512]{2,1,0:T(8,128)(2,1)}, u32[]{:S(2)}, u32[]{:S(2)}) %all-to-all-start.2) | async-done | bytes 2097184 | tf_op jit(solution)/shard_map/all_to_all | solution.py:77
  303.6 1.2 fusion.19
  304.8 1.8 fusion.18
  307.8 1.1 fusion.16
  310.4 9.2 %fusion.30 = f32[2048,512]{1,0:T(8,128)} fusion(bf16[2048,2048]{1,0:T(8,128)(2,1)S(1)} %bitcast.204, bf16[2048,512]{1,0:T(8,128)(2,1)} %bitcast.17), kind=kOutput, calls=%fused_computation.174 | convolution fusion | flops 4294967296 | bytes 14680064 | tf_op jit(solution)/shard_map/dot_general | solution.py:123
  319.6 7.5 %fusion.32 = f32[2048,512]{1,0:T(8,128)} fusion(bf16[2048,2048]{1,0:T(8,128)(2,1)S(1)} %bitcast.205, bf16[2048,512]{1,0:T(8,128)(2,1)} %collective-permute-done.1), kind=kOutput, calls=%fused_computation.176 | convolution fusion | flops 4294967296 | bytes 14680064 | tf_op jit(solution)/shard_map/dot_general | solution.py:124
  327.2 7.6 %fusion.31 = f32[2048,512]{1,0:T(8,128)} fusion(bf16[2048,2048]{1,0:T(8,128)(2,1)S(1)} %bitcast.206, bf16[2048,512]{1,0:T(8,128)(2,1)} %collective-permute-done), kind=kOutput, calls=%fused_computation.175 | convolution fusion | flops 4294967296 | bytes 14680064 | tf_op jit(solution)/shard_map/dot_general | solution.py:123
  334.8 16.1 %fusion.6 = f32[2048,2048]{1,0:T(8,128)} fusion(bf16[2048,512]{1,0:T(8,128)(2,1)} %bitcast.36, f32[2048,512]{1,0:T(8,128)} %fusion.30, bf16[2048,2048]{1,0:T(8,128)(2,1)} %bitcast.207, bf16[2048,512]{1,0:T(8,128)(2,1)S(1)} %bitcast.168, f32[2048]{0:T(1024)S(1)} %bitcast.214), kind=kOutput, calls=%fused_computation.18 | convolution fusion | flops 8597274624 | bytes 33562624 | tf_op jit(solution)/shard_map/rf,df->rd/dot_general | solution.py:126
  350.9 13.5 %add_convert_fusion = bf16[2048,2048]{1,0:T(8,128)(2,1)} fusion(f32[2048,2048]{1,0:T(8,128)} %fusion.6, bf16[2048,512]{1,0:T(8,128)(2,1)} %collective-permute-done.2, f32[2048,512]{1,0:T(8,128)} %fusion.32, f32[2048,512]{1,0:T(8,128)} %fusion.31, f32[2048]{0:T(1024)S(1)} %bitcast.215), kind=kOutput, calls=%fused_computation | convolution fusion | flops 4310695936 | bytes 35659776 | tf_op jit(solution)/shard_map/rf,df->rd/dot_general | solution.py:126
  377.2 1.2 slice_dynamic-update-slice_fusion.2
  378.4 1.1 constant_dynamic-update-slice_fusion.33
  380.6 1.3 copy-done.5
  381.9 1.5 fusion.33
  383.4 4.8 convolution_convert_fusion
  388.1 1.3 copy.30
  389.5 4.7 all_to_all.47
  394.3 71.6 %reduce-scatter.2.cloned.1.call-done = bf16[128,2048]{1,0:T(8,128)(2,1)} async-done(((bf16[2048,2048]{1,0:T(8,128)(2,1)}), bf16[128,2048]{1,0:T(8,128)(2,1)}) %reduce-scatter.2.cloned.1.call-update) | async-done | bytes 524304 | tf_op jit(solution)/shard_map/reduce_scatter | solution.py:128
  467.0 4.2 all_to_all.48
  472.1 3.0 copy.120
  475.2 1.3 copy.121
  476.5 3.0 copy.122
  (99 shorter events, 34.6 us)
Async XLA Ops:
  7.2 0.7 copy-start
  7.2 295.3 %all-gather.6.cloned.1.call-start = ((), (), s32[]{:S(2)}) async-start(), calls=%async_computation.7 | async-start | bytes 8912896 | tf_op jit(solution)/shard_map/all_gather | solution.py:61
  53.2 2.4 copy-start.8
  61.7 69.2 %all-to-all-start = ((bf16[16,128,512]{2,1,0:T(8,128)(2,1)}), bf16[16,128,512]{2,1,0:T(8,128)(2,1)}, u32[]{:S(2)}, u32[]{:S(2)}) async-start(bf16[16,128,512]{2,1,0:T(8,128)(2,1)} %get-tuple-element.57), calls=%async_computation | async-start | bytes 4194304 | tf_op jit(solution)/shard_map/all_to_all | solution.py:70
  130.9 87.5 %all-to-all-start.1 = ((bf16[16,1,128,512]{3,2,1,0:T(8,128)(2,1)}), bf16[16,1,128,512]{3,2,1,0:T(8,128)(2,1)S(1)}, u32[]{:S(2)}, u32[]{:S(2)}) async-start(bf16[16,1,128,512]{3,2,1,0:T(8,128)(2,1)} %constant_dynamic-update-slice_fusion.1), calls=%async_computation.1 | async-start | bytes 4194304 | tf_op jit(solution)/shard_map/all_to_all | solution.py:72
  149.9 92.6 %copy-start.3 = (f32[128,512]{1,0:T(8,128)S(1)}, f32[128,512]{1,0:T(8,128)}, u32[]{:S(2)}) copy-start(f32[128,512]{1,0:T(8,128)} %param.19) | copy-start | bytes 786436
  218.4 84.1 %all-to-all-start.2 = ((bf16[16,128,512]{2,1,0:T(8,128)(2,1)}), bf16[16,128,512]{2,1,0:T(8,128)(2,1)}, u32[]{:S(2)}, u32[]{:S(2)}) async-start(bf16[16,128,512]{2,1,0:T(8,128)(2,1)} %convert_element_type.59), calls=%async_computation.2 | async-start | bytes 4194304 | tf_op jit(solution)/shard_map/all_to_all | solution.py:77
  242.4 122.0 %all-gather.8.cloned.1.call-start = ((), (), s32[]{:S(2)}) async-start(), calls=%async_computation.8 | async-start | bytes 6684672 | tf_op jit(solution)/shard_map/all_gather | solution.py:88
  244.4 221.5 %reduce-scatter.2.cloned.1.call-start = ((), (), s32[]{:S(2)}) async-start(), calls=%async_computation.6 | async-start | bytes 8912896 | tf_op jit(solution)/shard_map/reduce_scatter | solution.py:128
  245.0 74.6 %collective-permute-start.1 = (bf16[2048,512]{1,0:T(8,128)(2,1)S(1)}, bf16[2048,512]{1,0:T(8,128)(2,1)}, u32[]{:S(2)}, u32[]{:S(2)}) collective-permute-start(bf16[2048,512]{1,0:T(8,128)(2,1)S(1)} %bitcast.167), channel_id=1, source_target_pairs={{0,1},{1,0},{2,3},{3,2},{4,5},{5,4},{6,7},{7,6},{8,9},{9,8},{10,11... | collective-permute-start | bytes 6291464 | tf_op jit(solution)/shard_map/ppermute | solution.py:120
  245.1 82.1 %collective-permute-start = (bf16[2048,512]{1,0:T(8,128)(2,1)}, bf16[2048,512]{1,0:T(8,128)(2,1)}, u32[]{:S(2)}, u32[]{:S(2)}) collective-permute-start(bf16[2048,512]{1,0:T(8,128)(2,1)} %bitcast.17), channel_id=1, source_target_pairs={{0,1},{1,0},{2,3},{3,2},{4,5},{5,4},{6,7},{7,6},{8,9},{9,8},{10,11... | collective-permute-start | bytes 6291464 | tf_op jit(solution)/shard_map/ppermute | solution.py:119
  302.5 48.4 %collective-permute-start.2 = (bf16[2048,512]{1,0:T(8,128)(2,1)}, bf16[2048,512]{1,0:T(8,128)(2,1)}, u32[]{:S(2)}, u32[]{:S(2)}) collective-permute-start(bf16[2048,512]{1,0:T(8,128)(2,1)} %bitcast.36), channel_id=1, source_target_pairs={{0,1},{1,0},{2,3},{3,2},{4,5},{5,4},{6,7},{7,6},{8,9},{9,8},{10,11... | collective-permute-start | bytes 6291464 | tf_op jit(solution)/shard_map/ppermute | solution.py:121
  303.5 3.1 slice-start
  303.6 6.4 %copy-start.2 = (bf16[2048,2048]{1,0:T(8,128)(2,1)S(1)}, bf16[2048,2048]{1,0:T(8,128)(2,1)}, u32[]{:S(2)}) copy-start(bf16[2048,2048]{1,0:T(8,128)(2,1)} %all-gather.6.cloned.1.call-done) | copy-start | bytes 25165828
  310.4 16.8 %copy-start.4 = (bf16[16,128,2048]{2,1,0:T(8,128)(2,1)}, bf16[16,128,2048]{2,1,0:T(8,128)(2,1)S(1)}, u32[]{:S(2)}) copy-start(bf16[16,128,2048]{2,1,0:T(8,128)(2,1)S(1)} %fusion.7) | copy-start | bytes 25165828
  380.5 1.3 copy-start.5
  380.6 2.8 copy-start.6
  380.6 2.8 copy-start.7
  475.2 4.4 copy-start.1
Sparse Core Ops, SparseCore 0:
  55.7 182.6 all-gather.5
  245.3 107.7 all-gather.7
  364.5 101.4 reduce-scatter.1
